TPU v7x, 32 devices: a whole 2x2x4 slice. The times are simulated.
32 devices in a mesh: grp: 2 (over x), sp: 4 (over z), tp: 4 (over y, core).
Axes of the slice: x: 2, y: 2, z: 4, core: 2. Of those that a mesh axis runs over, the one named last changes fastest.
Arguments:
- tokens: bfloat16 [1792, 4096], P(('grp', 'sp'), 'tp'), parts along dimension 0, may hold values from -130 to 130
- rms_gain: float32 [2, 4096], replicated, may hold values from 0.1 to 1.9
- w_value: bfloat16 [2, 4096, 2048], P(None, 'sp', 'tp'), may hold values from -0.09375 to 0.09375
- w_gate: bfloat16 [2, 4096, 2048], P(None, 'sp', 'tp'), may hold values from -0.09375 to 0.09375
- taps: float32 [2, 31, 2048], P(None, None, 'tp'), may hold values from -8 to 8
- ln_gain: float32 [2, 2048], P(None, 'tp'), may hold values from 0.1 to 1.9
- ln_bias: float32 [2, 2048], P(None, 'tp'), may hold values from -3 to 3
- w_out: bfloat16 [2, 2048, 4096], P(None, 'sp', 'tp'), may hold values from -0.125 to 0.125
Outputs:
- result: bfloat16 [1792, 4096], P(('grp', 'sp'), 'tp'), parts along dimension 0
There are 2 independent parts, one for each index of `grp`. A program takes and returns all parts, laid end to end along the dimension named above; an argument that names none is the same for every part. Nothing has to cross between parts.
All inputs are finite; a program needn't handle non-finite values.
Results may differ from a plain program's by a relative error of at most 0.009.
Values may be sent and summed in bfloat16 or wider, within the bound.
A program may use at most 64 MiB of HBM per device.

v0:
```python
import jax
import jax.numpy as jnp
from jax import lax
from jax.sharding import PartitionSpec as P

CH = 2048


def passed_along(block, axis, distance):
    devices = range(lax.axis_size(axis))
    route = [(i - distance, i) for i in devices if i - distance in devices]
    return lax.ppermute(block, axis, route)


def project_in(weight, columns):
    return lax.dot_general(
        weight, columns, (((0,), (1,)), ((), ())), preferred_element_type=jnp.float32
    )


def project_out(rows, weight):
    return lax.dot_general(
        rows, weight, (((0,), (0,)), ((), ())), preferred_element_type=jnp.float32
    )


def norm_rows(wide, gain):
    return (wide * lax.rsqrt(jnp.mean(wide * wide, axis=1, keepdims=True) + 1e-06) * gain).astype(
        jnp.bfloat16
    )


def shards(tokens, rms_gain, w_value, w_gate, taps, ln_gain, ln_bias, w_out):
    layers = w_value.shape[0]
    tok_rows = tokens.shape[0]
    chans = w_value.shape[2]
    reach = taps.shape[1]
    current = tokens
    for layer in range(layers):
        gain = rms_gain[layer]
        whole_rows = lax.all_gather(current, "tp", axis=1, tiled=True)
        normed = norm_rows(whole_rows.astype(jnp.float32), gain)
        value_t = project_in(lax.all_gather(w_value[layer], "sp", axis=0, tiled=True), normed)
        gate_t = project_in(lax.all_gather(w_gate[layer], "sp", axis=0, tiled=True), normed)
        glu_t = (value_t * jax.nn.sigmoid(gate_t)).astype(jnp.bfloat16)
        earlier = passed_along(glu_t[:, tok_rows - (reach - 1) :], "sp", 1)
        extended = jnp.concatenate([earlier, glu_t], axis=1).astype(jnp.float32)
        layer_taps = taps[layer]
        conv = jnp.zeros((chans, tok_rows), jnp.float32)
        for k in range(reach):
            conv = conv + layer_taps[k][:, None] * extended[:, k : k + tok_rows]
        total, total_sq = lax.psum((jnp.sum(conv, axis=0), jnp.sum(conv * conv, axis=0)), "tp")
        mean = total / CH
        var = total_sq / CH - mean * mean
        shaped = (conv - mean[None, :]) * lax.rsqrt(var + 1e-05)[None, :] * ln_gain[layer][
            :, None
        ] + ln_bias[layer][:, None]
        act_t = jax.nn.silu(shaped).astype(jnp.bfloat16)
        act_all = lax.all_gather(act_t, "tp", axis=0, tiled=True)
        branch = project_out(act_all, lax.all_gather(w_out[layer], "sp", axis=0, tiled=True))
        current = (current.astype(jnp.float32) + branch).astype(jnp.bfloat16)
    return current


def solution(mesh):
    return jax.shard_map(
        shards,
        mesh=mesh,
        in_specs=(
            P(("grp", "sp"), "tp"),
            P(),
            P(None, "sp", "tp"),
            P(None, "sp", "tp"),
            P(None, None, "tp"),
            P(None, "tp"),
            P(None, "tp"),
            P(None, "sp", "tp"),
        ),
        out_specs=P(("grp", "sp"), "tp"),
        check_vma=False,
    )
```

profile of v0, /device:TPU:0, one launch (start us, length us, event | category | flops | bytes accessed | tf_op | source)
XLA Modules:
  0.0 555.3 jit_solution(11916564640636365866)
XLA Ops:
  6.5 0.7 all-gather.15.cloned.1.call-update
  7.3 3.0 fusion.142
  10.4 1.5 fusion.141
  11.9 3.0 fusion.140
  15.2 17.5 %all-gather.15.cloned.1.call-done = bf16[224,4096]{1,0:T(8,128)(2,1)} async-done(((bf16[224,1024]{1,0:T(8,128)(2,1)}), bf16[224,4096]{1,0:T(8,128)(2,1)}) %all-gather.15.cloned.1.call-update) | async-done | bytes 1835024 | tf_op jit(solution)/shard_map/all_gather | solution.py:41
  32.8 1.9 fusion.12
  34.7 80.4 %all-gather.21.cloned.1.call-done = bf16[1,4096,512]{2,1,0:T(8,128)(2,1)} async-done(((bf16[1,1024,512]{2,1,0:T(8,128)(2,1)}), bf16[1,4096,512]{2,1,0:T(8,128)(2,1)}) %all-gather.21.cloned.1.call-update) | async-done | bytes 4194320 | tf_op jit(solution)/shard_map/all_gather | solution.py:44
  115.1 4.1 fusion.57
  119.2 76.7 %all-gather.19.cloned.1.call-done = bf16[1,4096,512]{2,1,0:T(8,128)(2,1)} async-done(((bf16[1,1024,512]{2,1,0:T(8,128)(2,1)}), bf16[1,4096,512]{2,1,0:T(8,128)(2,1)}) %all-gather.19.cloned.1.call-update) | async-done | bytes 4194320 | tf_op jit(solution)/shard_map/all_gather | solution.py:43
  195.9 3.3 fusion.66
  199.3 1.3 collective-permute-start
  200.6 1.6 collective-permute-done
  202.2 2.4 fusion.137
  204.6 6.3 %all-reduce.1 = (f32[224]{0:T(256)S(1)}, f32[224]{0:T(256)S(1)}) all-reduce(f32[224]{0:T(256)S(1)} %get-tuple-element.8, f32[224]{0:T(256)S(1)} %get-tuple-element.7), channel_id=1, replica_groups=mesh['grp'=2,'sp'=4,'tp'=4] {'tp'}, use_global_device_ids=true, to_apply=%region_4.0 | all-reduce | flops 448 | bytes 3584 | tf_op jit(solution)/shard_map/psum | solution.py:52
  211.2 9.1 %all_gather.33 = bf16[2048,224]{0,1:T(8,128)(2,1)S(1)} all-gather(bf16[512,224]{0,1:T(8,128)(2,1)S(1)} %multiply_convert_fusion.1), channel_id=1, replica_groups=mesh['grp'=2,'sp'=4,'tp'=4] {'tp'}, dimensions={0}, use_global_device_ids=true | all-gather | bytes 1146880 | tf_op jit(solution)/shard_map/all_gather | solution.py:59
  220.3 56.3 %all-gather.23.cloned.1.call-done = bf16[1,2048,1024]{2,1,0:T(8,128)(2,1)} async-done(((bf16[1,512,1024]{2,1,0:T(8,128)(2,1)}), bf16[1,2048,1024]{2,1,0:T(8,128)(2,1)}) %all-gather.23.cloned.1.call-update) | async-done | bytes 4194320 | tf_op jit(solution)/shard_map/all_gather | solution.py:60
  276.6 4.1 fusion.27
  281.4 0.7 all-gather.25.cloned.1.call-update
  282.1 0.7 all-gather.29.cloned.1.call-update
  282.8 17.7 %all-gather.17.cloned.1.call-done = bf16[224,4096]{1,0:T(8,128)(2,1)} async-done(((bf16[224,1024]{1,0:T(8,128)(2,1)}), bf16[224,4096]{1,0:T(8,128)(2,1)}) %all-gather.17.cloned.1.call-update) | async-done | bytes 1835024 | tf_op jit(solution)/shard_map/all_gather | solution.py:41
  300.5 1.9 fusion.15
  302.4 80.2 %all-gather.27.cloned.1.call-done = bf16[1,4096,512]{2,1,0:T(8,128)(2,1)} async-done(((bf16[1,1024,512]{2,1,0:T(8,128)(2,1)}), bf16[1,4096,512]{2,1,0:T(8,128)(2,1)}) %all-gather.27.cloned.1.call-update) | async-done | bytes 4194320 | tf_op jit(solution)/shard_map/all_gather | solution.py:44
  382.7 4.1 fusion.51
  386.8 76.7 %all-gather.25.cloned.1.call-done = bf16[1,4096,512]{2,1,0:T(8,128)(2,1)} async-done(((bf16[1,1024,512]{2,1,0:T(8,128)(2,1)}), bf16[1,4096,512]{2,1,0:T(8,128)(2,1)}) %all-gather.25.cloned.1.call-update) | async-done | bytes 4194320 | tf_op jit(solution)/shard_map/all_gather | solution.py:43
  463.5 3.3 fusion.69
  466.9 1.3 collective-permute-start.1
  468.2 1.5 collective-permute-done.1
  469.8 2.4 fusion.136
  472.2 6.3 %all-reduce = (f32[224]{0:T(256)S(1)}, f32[224]{0:T(256)S(1)}) all-reduce(f32[224]{0:T(256)S(1)} %get-tuple-element.6, f32[224]{0:T(256)S(1)} %get-tuple-element.5), channel_id=1, replica_groups=mesh['grp'=2,'sp'=4,'tp'=4] {'tp'}, use_global_device_ids=true, to_apply=%region_9.10 | all-reduce | flops 448 | bytes 3584 | tf_op jit(solution)/shard_map/psum | solution.py:52
  478.8 9.1 %all_gather.38 = bf16[2048,224]{0,1:T(8,128)(2,1)S(1)} all-gather(bf16[512,224]{0,1:T(8,128)(2,1)S(1)} %multiply_convert_fusion), channel_id=1, replica_groups=mesh['grp'=2,'sp'=4,'tp'=4] {'tp'}, dimensions={0}, use_global_device_ids=true | all-gather | bytes 1146880 | tf_op jit(solution)/shard_map/all_gather | solution.py:59
  487.9 56.5 %all-gather.29.cloned.1.call-done = bf16[1,2048,1024]{2,1,0:T(8,128)(2,1)} async-done(((bf16[1,512,1024]{2,1,0:T(8,128)(2,1)}), bf16[1,2048,1024]{2,1,0:T(8,128)(2,1)}) %all-gather.29.cloned.1.call-update) | async-done | bytes 4194320 | tf_op jit(solution)/shard_map/all_gather | solution.py:60
  544.3 4.1 fusion.24
  (48 shorter events, 1.8 us)
Async XLA Ops:
  6.5 3.9 copy-start
  6.5 26.2 %all-gather.15.cloned.1.call-start = ((), (), s32[]{:S(2)}) async-start(), calls=%async_computation | async-start | bytes 2293760 | tf_op jit(solution)/shard_map/all_gather | solution.py:41
  7.3 107.8 %all-gather.21.cloned.1.call-start = ((), (), s32[]{:S(2)}) async-start(), calls=%async_computation.3 | async-start | bytes 5242880 | tf_op jit(solution)/shard_map/all_gather | solution.py:44
  10.3 185.6 %all-gather.19.cloned.1.call-start = ((), (), s32[]{:S(2)}) async-start(), calls=%async_computation.2 | async-start | bytes 5242880 | tf_op jit(solution)/shard_map/all_gather | solution.py:43
  11.9 3.2 copy-start.7
  11.9 3.2 copy-start.5
  11.9 3.3 copy-start.6
  11.9 264.7 %all-gather.23.cloned.1.call-start = ((), (), s32[]{:S(2)}) async-start(), calls=%async_computation.4 | async-start | bytes 5242880 | tf_op jit(solution)/shard_map/all_gather | solution.py:60
  15.0 285.5 %all-gather.17.cloned.1.call-start = ((), (), s32[]{:S(2)}) async-start(), calls=%async_computation.1 | async-start | bytes 2293760 | tf_op jit(solution)/shard_map/all_gather | solution.py:41
  115.1 80.8 %copy-start.1 = (bf16[224,4096]{1,0:T(8,128)(2,1)S(1)}, bf16[224,4096]{1,0:T(8,128)(2,1)}, u32[]{:S(2)}) copy-start(bf16[224,4096]{1,0:T(8,128)(2,1)} %all-gather.15.cloned.1.call-done) | copy-start | bytes 5505028
  119.2 81.4 %copy-start.8 = (f32[2,512]{1,0:T(2,128)S(1)}, f32[2,512]{1,0:T(2,128)}, u32[]{:S(2)}) copy-start(f32[2,512]{1,0:T(2,128)} %param.14) | copy-start | bytes 12292
  199.3 2.9 collective-permute-start
  202.2 74.4 %copy-start.3 = (bf16[224,1024]{1,0:T(8,128)(2,1)S(1)}, bf16[224,1024]{1,0:T(8,128)(2,1)}, u32[]{:S(2)}) copy-start(bf16[224,1024]{1,0:T(8,128)(2,1)} %param.8) | copy-start | bytes 1376260
  280.7 101.9 %all-gather.27.cloned.1.call-start = ((), (), s32[]{:S(2)}) async-start(), calls=%async_computation.6 | async-start | bytes 5242880 | tf_op jit(solution)/shard_map/all_gather | solution.py:44
  281.3 182.2 %all-gather.25.cloned.1.call-start = ((), (), s32[]{:S(2)}) async-start(), calls=%async_computation.5 | async-start | bytes 5242880 | tf_op jit(solution)/shard_map/all_gather | solution.py:43
  282.1 262.3 %all-gather.29.cloned.1.call-start = ((), (), s32[]{:S(2)}) async-start(), calls=%async_computation.7 | async-start | bytes 5242880 | tf_op jit(solution)/shard_map/all_gather | solution.py:60
  382.7 80.8 %copy-start.2 = (bf16[224,4096]{1,0:T(8,128)(2,1)S(1)}, bf16[224,4096]{1,0:T(8,128)(2,1)}, u32[]{:S(2)}) copy-start(bf16[224,4096]{1,0:T(8,128)(2,1)} %all-gather.17.cloned.1.call-done) | copy-start | bytes 5505028
  466.9 2.9 collective-permute-start.1
  469.8 74.5 %copy-start.4 = (bf16[224,1024]{1,0:T(8,128)(2,1)S(1)}, bf16[224,1024]{1,0:T(8,128)(2,1)}, u32[]{:S(2)}) copy-start(bf16[224,1024]{1,0:T(8,128)(2,1)} %fusion.27) | copy-start | bytes 1376260
Sparse Core Ops, SparseCore 0:
  8.9 23.8 all-gather.14
  34.3 80.7 all-gather.20
  116.7 79.2 all-gather.18
  197.3 79.2 all-gather.22
  280.8 19.5 all-gather.16
  301.9 80.7 all-gather.26
  384.2 79.2 all-gather.24
  465.1 79.2 all-gather.28
where the time goes:
time: 556 us; the launch traced here: 555 us
  waiting for transfers between devices  468 us (84%)
  blocking collectives  30.7 us (6%)
  matrix products  23.1 us (4%)
  between operations  13.7 us (2%)
  other arithmetic  9.31 us (2%)
  local copies, waits for them, and re-layouts  7.75 us (1%)
    all_gather x2, waiting for transfers between devices, shards(): lax.all_gather(w_gate[layer], 'sp', axis=0, tiled=True)  161 us
    all_gather x2, waiting for transfers between devices, shards(): lax.all_gather(w_value[layer], 'sp', axis=0, tiled=True)  153 us
    all_gather x2, waiting for transfers between devices, shards(): lax.all_gather(w_out[layer], 'sp', axis=0, tiled=True)  113 us
    all_gather x2, waiting for transfers between devices, shards(): whole_rows = lax.all_gather(current, 'tp', axis=1, tiled=True)  35.2 us
    all_gather x2, blocking collectives, shards(): act_all = lax.all_gather(act_t, 'tp', axis=0, tiled=True)  18.2 us
    dot_general x4, matrix products, project_in(): lax.dot_general(weight, columns, (((0,), (1,)), ((), ())), preferred_elem...  14.9 us
    psum x2, blocking collectives, shards(): lax.psum((jnp.sum(conv, axis=0), jnp.sum(conv * conv, axis=0)), 'tp')  12.5 us
  transfers between devices with their start and end apart: 10, of which 10 were waited for; matrix products, arithmetic and copies ran while one was open for 6% of the time, Pallas kernels for 0%

commit v1 on v0

--- a/solution.py
+++ b/solution.py
@@ -1,9 +1,20 @@
+import functools
 import jax
 import jax.numpy as jnp
 from jax import lax
 from jax.sharding import PartitionSpec as P
+from jax.lax import all_to_all, axis_size
 
 CH = 2048
+
+
+def build_heads(matrix, k_dim, device_axis):
+    tall = jnp.stack([matrix for _ in range(axis_size(device_axis))], 0)
+    finding = all_to_all(tall, device_axis, 0, 0)
+    return jnp.concatenate(finding, k_dim)
+
+
+build_rounds = functools.partial(build_heads, k_dim=1, device_axis="tp")
 
 
 def passed_along(block, axis, distance):
@@ -38,7 +49,7 @@
     current = tokens
     for layer in range(layers):
         gain = rms_gain[layer]
-        whole_rows = lax.all_gather(current, "tp", axis=1, tiled=True)
+        whole_rows = build_rounds(current)
         normed = norm_rows(whole_rows.astype(jnp.float32), gain)
         value_t = project_in(lax.all_gather(w_value[layer], "sp", axis=0, tiled=True), normed)
         gate_t = project_in(lax.all_gather(w_gate[layer], "sp", axis=0, tiled=True), normed)

time: 556 us -> 508 us (0.914)
  waiting for transfers between devices: 468 us -> 384 us
  blocking collectives: 30.7 us -> 56.1 us
  local copies, waits for them, and re-layouts: 7.75 us -> 14.2 us
    all_gather x2, waiting for transfers between devices: 161 us -> 94.5 us  [shards(): lax.all_gather(w_gate[layer], 'sp', axis=0, tiled=True)]
    all_gather x2 -> x0, waiting for transfers between devices: 35.2 us -> none  [shards(): whole_rows = lax.all_gather(current, 'tp', axis=1, tiled=True)]
    all_to_all x0 -> x1, blocking collectives: none -> 25.4 us  [build_heads(): finding = all_to_all(tall, device_axis, 0, 0)]
    all_to_all x0 -> x1, waiting for transfers between devices: none -> 22.2 us  [build_heads(): finding = all_to_all(tall, device_axis, 0, 0)]
  transfers between devices with their start and end apart: 10 -> 9, of which waited for: 10 -> 9; matrix products, arithmetic and copies ran while one was open for 6% -> 8% of each run, Pallas kernels for 0% -> 0%
where the time goes in v1:
time: 508 us
  waiting for transfers between devices  384 us (76%)
  blocking collectives  56.1 us (11%)
  matrix products  25.4 us (5%)
  local copies, waits for them, and re-layouts  14.2 us (3%)
  between operations  13.7 us (3%)
  other arithmetic  7.1 us (1%)
  starting transfers between devices  7.01 us (1%)
    all_gather x2, waiting for transfers between devices, shards(): lax.all_gather(w_value[layer], 'sp', axis=0, tiled=True)  152 us
    all_gather x2, waiting for transfers between devices, shards(): lax.all_gather(w_out[layer], 'sp', axis=0, tiled=True)  111 us
    all_gather x2, waiting for transfers between devices, shards(): lax.all_gather(w_gate[layer], 'sp', axis=0, tiled=True)  94.5 us
    all_to_all x1, blocking collectives, build_heads(): finding = all_to_all(tall, device_axis, 0, 0)  25.4 us
    all_to_all x1, waiting for transfers between devices, build_heads(): finding = all_to_all(tall, device_axis, 0, 0)  22.2 us
    all_gather x2, blocking collectives, shards(): act_all = lax.all_gather(act_t, 'tp', axis=0, tiled=True)  18.2 us
    dot_general x4, matrix products, project_in(): lax.dot_general(weight, columns, (((0,), (1,)), ((), ())), preferred_elem...  18 us
    psum x2, blocking collectives, shards(): lax.psum((jnp.sum(conv, axis=0), jnp.sum(conv * conv, axis=0)), 'tp')  12.5 us
  transfers between devices with their start and end apart: 9, of which 9 were waited for; matrix products, arithmetic and copies ran while one was open for 8% of the time, Pallas kernels for 0%

profile of v1, /device:TPU:0, one launch (start us, length us, event | category | flops | bytes accessed | tf_op | source)
XLA Modules:
  0.0 508.0 jit_solution(2979847719748121921)
XLA Ops:
  6.5 3.2 fusion.134
  9.8 1.5 fusion.133
  11.4 3.1 fusion.132
  15.8 1.5 stack.4
  17.3 4.3 all-to-all-start
  21.5 0.6 all-gather.23.cloned.1.call-update
  22.3 22.2 %all-to-all-done = bf16[4,224,1024]{2,1,0:T(8,128)(2,1)S(1)} async-done(((bf16[4,224,1024]{2,1,0:T(8,128)(2,1)}), bf16[4,224,1024]{2,1,0:T(8,128)(2,1)S(1)}, u32[]{:S(2)}, u32[]{:S(2)}) %all-to-all-start) | async-done | bytes 1835040 | tf_op jit(solution)/shard_map/all_to_all | solution.py:13
  44.8 2.2 copy.11
  47.5 45.8 %all-gather.15.cloned.1.call-done = bf16[1,4096,512]{2,1,0:T(8,128)(2,1)} async-done(((bf16[1,1024,512]{2,1,0:T(8,128)(2,1)}), bf16[1,4096,512]{2,1,0:T(8,128)(2,1)}) %all-gather.15.cloned.1.call-update) | async-done | bytes 4194320 | tf_op jit(solution)/shard_map/all_gather | solution.py:55
  93.4 4.5 fusion.53
  97.9 76.3 %all-gather.13.cloned.1.call-done = bf16[1,4096,512]{2,1,0:T(8,128)(2,1)} async-done(((bf16[1,1024,512]{2,1,0:T(8,128)(2,1)}), bf16[1,4096,512]{2,1,0:T(8,128)(2,1)}) %all-gather.13.cloned.1.call-update) | async-done | bytes 4194320 | tf_op jit(solution)/shard_map/all_gather | solution.py:54
  174.2 4.5 fusion.62
  178.7 1.3 collective-permute-start
  180.0 1.6 collective-permute-done
  181.6 2.4 fusion.129
  184.0 6.3 %all-reduce.1 = (f32[224]{0:T(256)S(1)}, f32[224]{0:T(256)S(1)}) all-reduce(f32[224]{0:T(256)S(1)} %get-tuple-element.8, f32[224]{0:T(256)S(1)} %get-tuple-element.7), channel_id=1, replica_groups=mesh['grp'=2,'sp'=4,'tp'=4] {'tp'}, use_global_device_ids=true, to_apply=%region_4.0 | all-reduce | flops 448 | bytes 3584 | tf_op jit(solution)/shard_map/psum | solution.py:63
  190.6 9.1 %all_gather.26 = bf16[2048,224]{0,1:T(8,128)(2,1)S(1)} all-gather(bf16[512,224]{0,1:T(8,128)(2,1)S(1)} %multiply_convert_fusion.3), channel_id=1, replica_groups=mesh['grp'=2,'sp'=4,'tp'=4] {'tp'}, dimensions={0}, use_global_device_ids=true | all-gather | bytes 1146880 | tf_op jit(solution)/shard_map/all_gather | solution.py:70
  199.7 55.4 %all-gather.17.cloned.1.call-done = bf16[1,2048,1024]{2,1,0:T(8,128)(2,1)} async-done(((bf16[1,512,1024]{2,1,0:T(8,128)(2,1)}), bf16[1,2048,1024]{2,1,0:T(8,128)(2,1)}) %all-gather.17.cloned.1.call-update) | async-done | bytes 4194320 | tf_op jit(solution)/shard_map/all_gather | solution.py:71
  255.0 3.3 fusion.23
  258.6 25.4 %all_to_all.10 = bf16[4,224,1024]{2,1,0:T(8,128)(2,1)S(1)} all-to-all(bf16[4,224,1024]{2,1,0:T(8,128)(2,1)S(1)} %stack.5), channel_id=1, replica_groups=mesh['grp'=2,'sp'=4,'tp'=4] {'tp'}, dimensions={0} | all-to-all | bytes 3670016 | tf_op jit(solution)/shard_map/all_to_all | solution.py:13
  284.4 2.2 copy.12
  287.1 48.7 %all-gather.21.cloned.1.call-done = bf16[1,4096,512]{2,1,0:T(8,128)(2,1)} async-done(((bf16[1,1024,512]{2,1,0:T(8,128)(2,1)}), bf16[1,4096,512]{2,1,0:T(8,128)(2,1)}) %all-gather.21.cloned.1.call-update) | async-done | bytes 4194320 | tf_op jit(solution)/shard_map/all_gather | solution.py:55
  335.7 4.5 fusion.47
  340.3 76.1 %all-gather.19.cloned.1.call-done = bf16[1,4096,512]{2,1,0:T(8,128)(2,1)} async-done(((bf16[1,1024,512]{2,1,0:T(8,128)(2,1)}), bf16[1,4096,512]{2,1,0:T(8,128)(2,1)}) %all-gather.19.cloned.1.call-update) | async-done | bytes 4194320 | tf_op jit(solution)/shard_map/all_gather | solution.py:54
  416.4 4.5 fusion.65
  420.9 1.3 collective-permute-start.1
  422.2 1.5 collective-permute-done.1
  423.8 2.4 fusion.128
  426.2 6.3 %all-reduce = (f32[224]{0:T(256)S(1)}, f32[224]{0:T(256)S(1)}) all-reduce(f32[224]{0:T(256)S(1)} %get-tuple-element.6, f32[224]{0:T(256)S(1)} %get-tuple-element.5), channel_id=1, replica_groups=mesh['grp'=2,'sp'=4,'tp'=4] {'tp'}, use_global_device_ids=true, to_apply=%region_9.10 | all-reduce | flops 448 | bytes 3584 | tf_op jit(solution)/shard_map/psum | solution.py:63
  432.7 9.1 %all_gather.30 = bf16[2048,224]{0,1:T(8,128)(2,1)S(1)} all-gather(bf16[512,224]{0,1:T(8,128)(2,1)S(1)} %multiply_convert_fusion.2), channel_id=1, replica_groups=mesh['grp'=2,'sp'=4,'tp'=4] {'tp'}, dimensions={0}, use_global_device_ids=true | all-gather | bytes 1146880 | tf_op jit(solution)/shard_map/all_gather | solution.py:70
  441.8 55.2 %all-gather.23.cloned.1.call-done = bf16[1,2048,1024]{2,1,0:T(8,128)(2,1)} async-done(((bf16[1,512,1024]{2,1,0:T(8,128)(2,1)}), bf16[1,2048,1024]{2,1,0:T(8,128)(2,1)}) %all-gather.23.cloned.1.call-update) | async-done | bytes 4194320 | tf_op jit(solution)/shard_map/all_gather | solution.py:71
  497.1 4.1 fusion.20
  (45 shorter events, 4.0 us)
Async XLA Ops:
  6.5 3.3 copy-start
  6.5 86.8 %all-gather.15.cloned.1.call-start = ((), (), s32[]{:S(2)}) async-start(), calls=%async_computation.3 | async-start | bytes 5242880 | tf_op jit(solution)/shard_map/all_gather | solution.py:55
  9.8 164.4 %all-gather.13.cloned.1.call-start = ((), (), s32[]{:S(2)}) async-start(), calls=%async_computation.2 | async-start | bytes 5242880 | tf_op jit(solution)/shard_map/all_gather | solution.py:54
  11.3 4.4 copy-start.1
  11.4 243.7 %all-gather.17.cloned.1.call-start = ((), (), s32[]{:S(2)}) async-start(), calls=%async_computation.4 | async-start | bytes 5242880 | tf_op jit(solution)/shard_map/all_gather | solution.py:71
  14.6 321.2 %all-gather.21.cloned.1.call-start = ((), (), s32[]{:S(2)}) async-start(), calls=%async_computation.6 | async-start | bytes 5242880 | tf_op jit(solution)/shard_map/all_gather | solution.py:55
  15.1 401.3 %all-gather.19.cloned.1.call-start = ((), (), s32[]{:S(2)}) async-start(), calls=%async_computation.5 | async-start | bytes 5242880 | tf_op jit(solution)/shard_map/all_gather | solution.py:54
  15.7 6.4 %copy-start.2 = (f32[2,31,512]{2,0,1:T(2,128)S(1)}, f32[2,31,512]{2,0,1:T(2,128)}, u32[]{:S(2)}) copy-start(f32[2,31,512]{2,0,1:T(2,128)} %param.12) | copy-start | bytes 380932
  15.7 6.4 %copy-start.4 = (f32[2,512]{1,0:T(2,128)S(1)}, f32[2,512]{1,0:T(2,128)}, u32[]{:S(2)}) copy-start(f32[2,512]{1,0:T(2,128)} %param.13) | copy-start | bytes 12292
  15.8 6.5 %copy-start.3 = (f32[2,4096]{1,0:T(2,128)S(1)}, f32[2,4096]{1,0:T(2,128)}, u32[]{:S(2)}) copy-start(f32[2,4096]{1,0:T(2,128)} %param.9) | copy-start | bytes 98308
  17.3 27.2 %all-to-all-start = ((bf16[4,224,1024]{2,1,0:T(8,128)(2,1)}), bf16[4,224,1024]{2,1,0:T(8,128)(2,1)S(1)}, u32[]{:S(2)}, u32[]{:S(2)}) async-start(bf16[4,224,1024]{2,1,0:T(8,128)(2,1)} %stack.4), calls=%async_computation | async-start | bytes 3670016 | tf_op jit(solution)/shard_map/all_to_all | solution.py:13
  21.5 475.5 %all-gather.23.cloned.1.call-start = ((), (), s32[]{:S(2)}) async-start(), calls=%async_computation.7 | async-start | bytes 5242880 | tf_op jit(solution)/shard_map/all_gather | solution.py:71
  97.9 82.1 %copy-start.5 = (f32[2,512]{1,0:T(2,128)S(1)}, f32[2,512]{1,0:T(2,128)}, u32[]{:S(2)}) copy-start(f32[2,512]{1,0:T(2,128)} %param.14) | copy-start | bytes 12292
  178.7 2.9 collective-permute-start
  420.9 2.9 collective-permute-start.1
Sparse Core Ops, SparseCore 0:
  9.9 83.4 all-gather.14
  94.9 79.2 all-gather.12
  175.8 79.2 all-gather.16
  256.5 79.2 all-gather.20
  337.1 79.2 all-gather.18
  417.8 79.2 all-gather.22
